TPU v7x, 512 devices: a whole 4x8x8 slice. The times are simulated.
512 devices in a mesh: ep: 32 (over z, x), tp: 16 (over y, core).
Axes of the slice: x: 4, y: 8, z: 8, core: 2. Of those that a mesh axis runs over, the one named last changes fastest.
Arguments:
- mix_rows: bfloat16 [8192, 2048], P('ep'), may hold values from -6 to 6
- mix_gain: bfloat16 [2048], replicated, may hold values from 0.099609375 to 1.8984375
- w_query: bfloat16 [1024, 2048], P('tp'), may hold values from -0.125 to 0.125
- w_key: bfloat16 [1024, 2048], P('tp'), may hold values from -0.125 to 0.125
- w_value: bfloat16 [1024, 2048], P('tp'), may hold values from -0.125 to 0.125
- key_offset: float32 [16, 8192], P('tp'), may hold values from -11 to 0
- w_out: bfloat16 [1024, 2048], P('tp'), may hold values from -0.1875 to 0.1875
- out_gain: bfloat16 [2048], replicated, may hold values from 0.099609375 to 1.8984375
- exp_rows: bfloat16 [3072, 2048], P('ep', 'tp'), may hold values from -100 to 100
- exp_gain: bfloat16 [2048], P('tp'), may hold values from 0.099609375 to 1.8984375
- routes: int32 [3072, 4], P('ep'), may hold values from 0 to 31, all different within a row; in each aligned block of 96 rows (0 to 95, 96 to 191, ...) at most 16 rows name the same one
- route_weight: float32 [3072, 4], P('ep'), may hold values from 0.05 to 1
- w_gate: bfloat16 [32, 2048, 2048], P('ep', None, 'tp'), may hold values from -0.5 to 0.5
- w_up: bfloat16 [32, 2048, 2048], P('ep', None, 'tp'), may hold values from -0.5 to 0.5
- w_down: bfloat16 [32, 2048, 2048], P('ep', 'tp'), may hold values from -0.1875 to 0.1875
Outputs:
- mix_out: bfloat16 [8192, 2048], P('ep')
- exp_out: bfloat16 [3072, 2048], P('ep', 'tp')
Inputs may be any that keep to these rules, and one draw needn't show every extreme that they name: `routes`: each row names 4 different experts. Within the rows of one device (aligned blocks of 96 rows) no expert is named by more than 16 rows, and in some blocks one expert is named by exactly 16 rows.
All inputs are finite; a program needn't handle non-finite values.
Results may differ from a plain program's by a relative error of at most 0.019.
Values may be sent and summed in bfloat16 or wider, within the bound.
No kernel may reach another device: no remote copies, remote signals or barrier semaphores. Data moves between devices by JAX's collectives and lax.ppermute only.
A program may use at most 128 MiB of HBM per device.

v0:
```python
import math
import jax
import jax.numpy as jnp
from jax import lax
from jax.sharding import Mesh
from jax.sharding import PartitionSpec as P

EP = ("ep_0", "ep_1")
TP = ("tp_0", "tp_1")
EPSILON = 1e-06
CLAMP_LIMIT = 7.0
SILU_SHARPNESS = 1.702


def gathered_by_axis(value, axes, dim):
    out = value
    for number in range(len(axes) - 1, -1, -1):
        out = lax.all_gather(out, axes[number], axis=dim, tiled=True)
    return out


def split_up(value, dim, devices):
    dims = value.shape
    tiles = value.reshape(*dims[:dim], devices, dims[dim] // devices, *dims[dim + 1 :])
    return jnp.moveaxis(tiles, dim, 0)


def sent_and_summed(value, axis, dim):
    devices = lax.axis_size(axis)
    tiles = lax.all_to_all(split_up(value, dim, devices), axis, 0, 0, tiled=True)
    return jnp.sum(tiles.astype(jnp.float32), axis=0)


def from_everyone(value, axis):
    copies = jnp.broadcast_to(value, (lax.axis_size(axis), *value.shape))
    return lax.all_to_all(copies, axis, split_axis=0, concat_axis=0, tiled=True)


def of_everyone(value, axis):
    return from_everyone(value, axis).sum(axis=0)


def gather_turned(arrays, axis, dims):
    turned = [jnp.moveaxis(a, dim, 0) for a, dim in zip(arrays, dims)]
    widths = [t[0].size for t in turned]
    both = jnp.concatenate([t.reshape(-1, w) for t, w in zip(turned, widths)], axis=1)
    out = lax.all_gather(both, axis, axis=0, tiled=True)
    tiles = jnp.split(out, [sum(widths[:k]) for k in range(1, len(widths))], axis=1)
    return tuple(
        (
            jnp.moveaxis(b.reshape(-1, *t.shape[1:]), 0, dim)
            for b, t, dim in zip(tiles, turned, dims)
        )
    )


def summed_rows_2(value, chips, core, dim):
    sizes = (lax.axis_size(chips), lax.axis_size(core))
    tiles = split_up(value, dim, sizes[0] * sizes[1])
    inside = tiles.shape[1:]
    tiles = tiles.reshape(*sizes, *inside).swapaxes(0, 1).reshape(-1, *inside)
    tiles = lax.psum_scatter(tiles, core, scatter_dimension=0, tiled=True)
    return lax.psum_scatter(tiles, chips, scatter_dimension=0, tiled=True)[0]


def normalize(numbers, gain):
    factor = lax.rsqrt(jnp.mean(numbers * numbers, axis=-1, keepdims=True) + EPSILON)
    return numbers * factor * gain.astype(jnp.float32)


def project(normed, weight):
    product = lax.dot_general(
        normed, weight, (((1,), (1,)), ((), ())), preferred_element_type=jnp.float32
    )
    return product.astype(jnp.bfloat16)


def gated_units(gate_pre, up_pre):
    gate_part = jnp.minimum(gate_pre, CLAMP_LIMIT)
    up_part = jnp.clip(up_pre, -CLAMP_LIMIT, CLAMP_LIMIT)
    return (up_part + 1.0) * (gate_part * jax.nn.sigmoid(SILU_SHARPNESS * gate_part))


def stick_terms(queries, block_pairs, offset_values, query_index, key_index):
    heads_here = queries.shape[1]
    head_size = queries.shape[2]
    width = heads_here * head_size
    key_rows = block_pairs[:, :width].reshape(-1, heads_here, head_size)
    value_rows = block_pairs[:, width:].reshape(-1, heads_here, head_size)
    scores = jnp.einsum(
        "thd,shd->hts", queries, key_rows, preferred_element_type=jnp.float32
    ) / math.sqrt(head_size)
    scores = scores + offset_values[:, None, :]
    visible = (key_index[None, :] < query_index[:, None])[None]
    keep_log = jnp.where(visible, jax.nn.log_sigmoid(-scores), 0.0)
    later_sum = lax.cumsum(keep_log, axis=2, reverse=True) - keep_log
    exponent = jax.nn.log_sigmoid(scores) + later_sum
    weights = jnp.where(visible, jnp.exp(exponent), 0.0).astype(jnp.bfloat16)
    attended = jnp.einsum("hts,shd->thd", weights, value_rows, preferred_element_type=jnp.float32)
    return (attended, jnp.sum(keep_log, axis=2))


def on_device(
    mix_rows,
    mix_gain,
    w_query,
    w_key,
    w_value,
    key_offset,
    w_out,
    out_gain,
    exp_rows,
    exp_gain,
    routes,
    route_weight,
    w_gate,
    w_up,
    w_down,
):
    row_count = mix_rows.shape[0]
    heads_here = key_offset.shape[0]
    head_size = w_query.shape[0] // heads_here
    normed = normalize(mix_rows.astype(jnp.float32), mix_gain).astype(jnp.bfloat16)
    queries = project(normed, w_query).reshape(row_count, heads_here, head_size)
    own_pairs = jnp.concatenate([project(normed, w_key), project(normed, w_value)], axis=1)
    own_start = lax.axis_index(EP) * row_count
    query_index = own_start + jnp.arange(row_count, dtype=jnp.int32)
    every_pair = gathered_by_axis(own_pairs, EP, 0)
    key_index = jnp.arange(every_pair.shape[0], dtype=jnp.int32)
    attended, _ = stick_terms(queries, every_pair, key_offset, query_index, key_index)
    attended = attended.reshape(row_count, heads_here * head_size).astype(jnp.bfloat16)
    tp_count = lax.axis_size(TP)
    model_width = w_out.shape[1]
    column_count = model_width // tp_count
    columns = w_out
    share = sent_and_summed(
        lax.dot_general(
            columns, attended, (((0,), (1,)), ((), ())), preferred_element_type=jnp.float32
        ).astype(jnp.bfloat16),
        TP,
        0,
    )
    row_sums = of_everyone(jnp.sum(share * share, axis=0), TP)
    factor = lax.rsqrt(row_sums / model_width + EPSILON)
    gain_share = lax.dynamic_slice_in_dim(
        out_gain, lax.axis_index(TP) * column_count, column_count, 0
    ).astype(jnp.float32)
    own_columns = (share.T * factor[:, None] * gain_share[None, :]).astype(jnp.bfloat16)
    mix_out = lax.all_gather(own_columns, TP, axis=1, tiled=True)
    token_count, top_count = routes.shape
    ep_count = lax.axis_size(EP)
    experts = w_gate.shape[0] * ep_count
    capacity = 4 * token_count * top_count // (3 * experts)
    route_list = routes.reshape(-1)
    matches = (route_list[:, None] == jnp.arange(experts, dtype=jnp.int32)[None, :]).astype(
        jnp.int32
    )
    earlier = jnp.cumsum(matches, axis=0) - matches
    slot_index = route_list * capacity + jnp.sum(earlier * matches, axis=1)
    token_of = jnp.arange(route_list.shape[0], dtype=jnp.int32) // top_count + 1
    owners = jnp.zeros((experts * capacity,), jnp.int32).at[slot_index].set(token_of)
    whole_rows, whole_gain = gather_turned((exp_rows, exp_gain), TP, (1, 0))
    normed_exp = normalize(whole_rows.astype(jnp.float32), whole_gain).astype(jnp.bfloat16)
    outgoing = jnp.where(
        owners[:, None] > 0, normed_exp[jnp.maximum(owners - 1, 0)], jnp.zeros((), jnp.bfloat16)
    )
    arrived = lax.all_to_all(outgoing, EP, split_axis=0, concat_axis=0, tiled=True)
    gate_pre = jnp.dot(arrived, w_gate[0], preferred_element_type=jnp.float32)
    up_pre = jnp.dot(arrived, w_up[0], preferred_element_type=jnp.float32)
    hidden = gated_units(gate_pre, up_pre).astype(jnp.bfloat16)
    columns = w_down[0]
    expert_out = (
        summed_rows_2(
            lax.dot_general(
                columns, hidden, (((0,), (1,)), ((), ())), preferred_element_type=jnp.float32
            ).astype(jnp.bfloat16),
            "tp_0",
            "tp_1",
            0,
        )
        .astype(jnp.float32)
        .astype(jnp.bfloat16)
    )
    returned = lax.all_to_all(expert_out, EP, split_axis=1, concat_axis=1, tiled=True)
    picked = (
        jnp.take(returned, slot_index, axis=1)
        .astype(jnp.float32)
        .reshape(-1, token_count, top_count)
    )
    combined = jnp.sum(picked * route_weight[None], axis=2)
    exp_out = combined.T.astype(jnp.bfloat16)
    return (mix_out, exp_out)


def solution(mesh):
    torus = Mesh(mesh.devices.reshape(8, 4, 8, 2), ("ep_0", "ep_1", "tp_0", "tp_1"))
    in_specs = (
        P(EP, None),
        P(),
        P(TP, None),
        P(TP, None),
        P(TP, None),
        P(TP, None),
        P(TP, None),
        P(),
        P(EP, TP),
        P(TP),
        P(EP, None),
        P(EP, None),
        P(EP, None, TP),
        P(EP, None, TP),
        P(EP, TP, None),
    )
    out_specs = (P(EP, None), P(EP, TP))
    return jax.shard_map(
        on_device, mesh=torus, in_specs=in_specs, out_specs=out_specs, check_vma=False
    )
```

profile of v0, /device:TPU:1, one launch (start us, length us, event | category | flops | bytes accessed | tf_op | source)
XLA Modules:
  0.0 288.5 jit_solution(9969811278149230020)
XLA Ops:
  8.1 1.6 fusion.13
  10.3 1.8 convolution_convert_fusion.3
  12.1 1.8 convolution_convert_fusion.4
  13.9 11.3 %all_gather.12 = bf16[1024,128]{0,1:T(8,128)(2,1)} all-gather(bf16[256,128]{0,1:T(8,128)(2,1)S(1)} %pad_maximum_fusion), channel_id=1, replica_groups=mesh['ep_0'=8,'ep_1'=4,'tp_0'=8,'tp_1'=2] {'ep_1'}, dimensions={0}, use_global_device_ids=true | all-gather | bytes 327680 | tf_op jit(solution)/shard_map/all_gather | solution.py:18
  28.4 2.9 %scatter_custom_fusion = s32[512]{0:T(512)S(1)} fusion(s32[384]{0:T(512)S(1)} %fusion.55, s32[384]{0:T(512)S(1)} %fusion.51, s32[]{:T(128)} %constant.94.clone.1), kind=kCustom, calls=%fused_computation.97 | custom fusion | bytes 2052 | tf_op jit(solution)/shard_map/scatter | solution.py:161
  32.1 23.8 %all_gather.15 = bf16[2048,97]{0,1:T(8,128)(2,1)S(1)} all-gather(bf16[128,97]{0,1:T(8,128)(2,1)S(1)} %pad_maximum_fusion.1), channel_id=1, replica_groups=mesh['ep_0'=8,'ep_1'=4,'tp_0'=8,'tp_1'=2] {'tp_0','tp_1'}, dimensions={0}, use_global_device_ids=true | all-gather | bytes 422144 | tf_op jit(solution)/shard_map/all_gather | solution.py:47
  56.3 2.5 gather_fusion
  58.8 1.5 broadcast_select_fusion
  60.3 10.9 %all-to-all-start.2 = ((bf16[32,16,2048]{2,1,0:T(8,128)(2,1)}), bf16[32,16,2048]{2,1,0:T(8,128)(2,1)S(1)}, u32[]{:S(2)}, u32[]{:S(2)}) async-start(bf16[32,16,2048]{2,1,0:T(8,128)(2,1)} %broadcast_select_fusion), calls=%async_computation.2 | async-start | bytes 4194304 | tf_op jit(solution)/shard_map/all_to_all | solution.py:167
  72.3 7.1 %fusion = f32[256,8192]{1,0:T(8,128)} fusion(f32[8192]{0:T(1024)S(1)} %bitcast.114, bf16[64,2048]{1,0:T(8,128)(2,1)S(1)} %copy-done.5, bf16[8192,128]{0,1:T(8,128)(2,1)} %all-gather.3.cloned.1.call-done, bf16[256,2048]{1,0:T(8,128)(2,1)} %param.15, f32[2048]{0:T(1024)S(1)} %convert_element_type.101, f32[256]{0:T(256)S(1)} %add_rsqrt_fusion.1), kind=kOutput, calls=%fused_computation.6 | convolution fusion | flops 341852160 | bytes 10789888 | tf_op jit(solution)/shard_map/thd,shd->hts/dot_general | solution.py:90
  79.4 7.4 %fusion.9 = f32[32,8,64,128]{3,1,2,0:T(8,128)S(1)} fusion(f32[256,8192]{1,0:T(8,128)} %fusion, s32[256]{0:T(256)S(1)} %iota_add_fusion), kind=kLoop, calls=%fused_computation.17 | loop fusion | flops 18874368 | bytes 16778240
  86.8 4.8 %copy.93 = f32[32,8,64,128]{3,2,1,0:T(8,128)} copy(f32[32,8,64,128]{3,1,2,0:T(8,128)S(1)} %fusion.9) | data formatting | bytes 16777216
  91.7 9.3 %copy.76 = f32[1,256,64,128]{1,2,3,0:T(8,128)} copy(f32[1,256,64,128]{3,2,1,0:T(8,128)} %bitcast.105) | data formatting | bytes 16777216 | tf_op jit(solution)/shard_map/reshape
  101.0 20.7 %all-to-all-done.2 = bf16[32,16,2048]{2,1,0:T(8,128)(2,1)S(1)} async-done(((bf16[32,16,2048]{2,1,0:T(8,128)(2,1)}), bf16[32,16,2048]{2,1,0:T(8,128)(2,1)S(1)}, u32[]{:S(2)}, u32[]{:S(2)}) %all-to-all-start.2) | async-done | bytes 2097184 | tf_op jit(solution)/shard_map/all_to_all | solution.py:167
  122.3 4.7 %fusion.12 = bf16[2048,512]{0,1:T(8,128)(2,1)} fusion(bf16[512,2048]{1,0:T(8,128)(2,1)S(1)} %bitcast.107, bf16[1,128,2048]{2,1,0:T(8,128)(2,1)S(1)} %copy-done, bf16[1,2048,128]{2,1,0:T(8,128)(2,1)} %param.28, f32[512,128]{1,0:T(8,128)S(1)} %convolution_minimum_fusion), kind=kOutput, calls=%fused_computation.20 | convolution fusion | flops 538509312 | bytes 5505024 | tf_op jit(solution)/shard_map/dot_general | solution.py:174
  127.0 3.2 %reshape_reshape.3 = bf16[8,2,128,512]{2,1,0,3:T(2,128)(2,1)S(1)} reshape(bf16[2048,512]{0,1:T(8,128)(2,1)} %fusion.12) | data formatting | bytes 4194304 | tf_op jit(solution)/shard_map/reshape;reshape | solution.py:61
  130.3 4.7 %copy.87 = bf16[8,2,128,512]{3,2,0,1:T(8,128)(2,1)} copy(bf16[8,2,128,512]{2,1,0,3:T(2,128)(2,1)S(1)} %reshape_reshape.3) | data formatting | bytes 4194304 | tf_op jit(solution)/shard_map/reshape;reshape | solution.py:61
  135.1 24.0 %fusion.67 = f32[1,256,64,128]{1,2,3,0:T(8,128)} fusion(f32[1,256,64,128]{1,2,3,0:T(8,128)} %copy.76), kind=kOutput, calls=%fused_computation.110 | output fusion | flops 266338304 | bytes 16777216 | tf_op jit(solution)/shard_map/reduce-window
  159.1 9.0 %copy.77 = f32[1,256,64,128]{3,2,1,0:T(8,128)} copy(f32[1,256,64,128]{1,2,3,0:T(8,128)} %fusion.67) | data formatting | bytes 16777216 | tf_op jit(solution)/shard_map/reduce-window
  169.7 2.3 broadcast.140
  172.0 1.0 copy-done.2
  173.0 18.7 %fusion.23 = bf16[256,64]{0,1:T(8,128)(2,1)S(1)} fusion(f32[32,8,64,128]{3,2,1,0:T(8,128)S(1)} %bitcast.110, f32[32,8,64,128]{3,2,1,0:T(8,128)S(1)} %bitcast.109, f32[256,8192]{1,0:T(8,128)} %fusion, s32[256]{0:T(256)S(1)} %iota_add_fusion, bf16[8192,128]{0,1:T(8,128)(2,1)S(1)} %copy-done.3), kind=kOutput, calls=%fused_computation.39 | convolution fusion | flops 314589184 | bytes 26248192 | tf_op jit(solution)/shard_map/hts,shd->thd/dot_general | solution.py:99
  192.3 1.2 copy.110
  193.5 6.5 %all-to-all-start = ((bf16[16,128,256]{1,2,0:T(8,128)(2,1)}), bf16[16,128,256]{1,2,0:T(8,128)(2,1)S(1)}, u32[]{:S(2)}, u32[]{:S(2)}) async-start(bf16[16,128,256]{1,2,0:T(8,128)(2,1)} %bitcast.102), calls=%async_computation | async-start | bytes 2097152 | tf_op jit(solution)/shard_map/all_to_all | solution.py:30
  200.6 30.3 %all-to-all-done = bf16[16,128,256]{1,2,0:T(8,128)(2,1)S(1)} async-done(((bf16[16,128,256]{1,2,0:T(8,128)(2,1)}), bf16[16,128,256]{1,2,0:T(8,128)(2,1)S(1)}, u32[]{:S(2)}, u32[]{:S(2)}) %all-to-all-start) | async-done | bytes 1048608 | tf_op jit(solution)/shard_map/all_to_all | solution.py:30
  231.8 4.2 %all-to-all-start.1 = ((f32[16,1,256]{2,1,0:T(1,128)}), f32[16,1,256]{2,1,0:T(1,128)S(1)}, u32[]{:S(2)}, u32[]{:S(2)}) async-start(f32[16,1,256]{2,1,0:T(1,128)} %broadcast_in_dim.31), calls=%async_computation.1 | async-start | bytes 32768 | tf_op jit(solution)/shard_map/all_to_all | solution.py:36
  236.8 6.6 %all-to-all-done.1 = f32[16,1,256]{2,1,0:T(1,128)S(1)} async-done(((f32[16,1,256]{2,1,0:T(1,128)}), f32[16,1,256]{2,1,0:T(1,128)S(1)}, u32[]{:S(2)}, u32[]{:S(2)}) %all-to-all-start.1) | async-done | bytes 16416 | tf_op jit(solution)/shard_map/all_to_all | solution.py:36
  244.3 1.7 copy.88
  246.0 6.3 %all-to-all-start.3 = ((bf16[128,32,16]{0,2,1:T(8,128)(2,1)}), bf16[128,32,16]{0,2,1:T(8,128)(2,1)S(1)}, u32[]{:S(2)}, u32[]{:S(2)}) async-start(bf16[128,32,16]{0,2,1:T(8,128)(2,1)} %bitcast.21), calls=%async_computation.5 | async-start | bytes 262144 | tf_op jit(solution)/shard_map/all_to_all | solution.py:184
  252.7 23.3 %all-gather.5.cloned.1.call-done = bf16[256,2048]{1,0:T(8,128)(2,1)} async-done(((bf16[256,128]{1,0:T(8,128)(2,1)}), bf16[256,2048]{1,0:T(8,128)(2,1)}) %all-gather.5.cloned.1.call-update) | async-done | bytes 1048592 | tf_op jit(solution)/shard_map/all_gather | solution.py:149
  276.0 1.4 gather_fusion.1
  278.4 2.3 copy.112
  (77 shorter events, 13.4 us)
Async XLA Ops:
  8.0 114.3 %copy-start = (bf16[1,128,2048]{2,1,0:T(8,128)(2,1)S(1)}, bf16[1,128,2048]{2,1,0:T(8,128)(2,1)}, u32[]{:S(2)}) copy-start(bf16[1,128,2048]{2,1,0:T(8,128)(2,1)} %param.29) | copy-start | bytes 1572868
  8.0 64.3 %all-gather.3.cloned.1.call-start = ((), (), s32[]{:S(2)}) async-start(), calls=%async_computation.6 | async-start | bytes 2359296 | tf_op jit(solution)/shard_map/all_gather | solution.py:18
  58.8 13.5 %copy-start.5 = (bf16[64,2048]{1,0:T(8,128)(2,1)S(1)}, bf16[64,2048]{1,0:T(8,128)(2,1)}, u32[]{:S(2)}) copy-start(bf16[64,2048]{1,0:T(8,128)(2,1)} %param.17) | copy-start | bytes 786436
  58.8 13.5 %copy-start.7 = (f32[1,8192]{1,0:T(1,128)S(1)}, f32[1,8192]{1,0:T(1,128)}, u32[]{:S(2)}) copy-start(f32[1,8192]{1,0:T(1,128)} %param.20) | copy-start | bytes 98308
  60.3 61.3 %all-to-all-start.2 = ((bf16[32,16,2048]{2,1,0:T(8,128)(2,1)}), bf16[32,16,2048]{2,1,0:T(8,128)(2,1)S(1)}, u32[]{:S(2)}, u32[]{:S(2)}) async-start(bf16[32,16,2048]{2,1,0:T(8,128)(2,1)} %broadcast_select_fusion), calls=%async_computation.2 | async-start | bytes 4194304 | tf_op jit(solution)/shard_map/all_to_all | solution.py:167
  71.2 128.9 %reduce-scatter.3.cloned.1.call-start = ((), (), s32[]{:S(2)}) async-start(), calls=%async_computation.8 | async-start | bytes 3145728 | tf_op jit(solution)/shard_map/reduce_scatter | solution.py:62
  91.7 29.9 %copy-start.4 = (bf16[1,2048,128]{2,1,0:T(8,128)(2,1)S(1)}, bf16[1,2048,128]{2,1,0:T(8,128)(2,1)}, u32[]{:S(2)}) copy-start(bf16[1,2048,128]{2,1,0:T(8,128)(2,1)} %param.27) | copy-start | bytes 1572868
  159.1 12.9 %copy-start.3 = (bf16[8192,128]{0,1:T(8,128)(2,1)S(1)}, bf16[8192,128]{0,1:T(8,128)(2,1)}, u32[]{:S(2)}) copy-start(bf16[8192,128]{0,1:T(8,128)(2,1)} %all-gather.3.cloned.1.call-done) | copy-start | bytes 6291460
  169.6 3.4 %copy-start.2 = (f32[1,256,64,128]{3,2,1,0:T(8,128)S(1)}, f32[1,256,64,128]{3,2,1,0:T(8,128)}, u32[]{:S(2)}) copy-start(f32[1,256,64,128]{3,2,1,0:T(8,128)} %copy.77) | copy-start | bytes 25165828
  173.0 18.7 %copy-start.6 = (bf16[64,2048]{1,0:T(8,128)(2,1)S(1)}, bf16[64,2048]{1,0:T(8,128)(2,1)}, u32[]{:S(2)}) copy-start(bf16[64,2048]{1,0:T(8,128)(2,1)} %param.21) | copy-start | bytes 786436
  173.0 107.6 %copy-start.1 = (bf16[1,128,2048]{2,1,0:T(8,128)(2,1)S(1)}, bf16[1,128,2048]{2,1,0:T(8,128)(2,1)}, u32[]{:S(2)}) copy-start(bf16[1,128,2048]{2,1,0:T(8,128)(2,1)} %param.29) | copy-start | bytes 1572868
  191.8 60.6 %copy-start.8 = (s32[96,4]{0,1:T(4,128)S(1)}, s32[96,4]{0,1:T(4,128)}, u32[]{:S(2)}) copy-start(s32[96,4]{0,1:T(4,128)} %param.25) | copy-start | bytes 4612
  191.8 60.7 %copy-start.9 = (f32[96,4]{0,1:T(4,128)S(1)}, f32[96,4]{0,1:T(4,128)}, u32[]{:S(2)}) copy-start(f32[96,4]{0,1:T(4,128)} %param.26) | copy-start | bytes 4612
  193.5 37.4 %all-to-all-start = ((bf16[16,128,256]{1,2,0:T(8,128)(2,1)}), bf16[16,128,256]{1,2,0:T(8,128)(2,1)S(1)}, u32[]{:S(2)}, u32[]{:S(2)}) async-start(bf16[16,128,256]{1,2,0:T(8,128)(2,1)} %bitcast.102), calls=%async_computation | async-start | bytes 2097152 | tf_op jit(solution)/shard_map/all_to_all | solution.py:30
  200.0 44.4 %reduce-scatter.5.cloned.1.call-start = ((), (), s32[]{:S(2)}) async-start(), calls=%async_computation.9 | async-start | bytes 1179648 | tf_op jit(solution)/shard_map/reduce_scatter | solution.py:63
  231.8 11.6 %all-to-all-start.1 = ((f32[16,1,256]{2,1,0:T(1,128)}), f32[16,1,256]{2,1,0:T(1,128)S(1)}, u32[]{:S(2)}, u32[]{:S(2)}) async-start(f32[16,1,256]{2,1,0:T(1,128)} %broadcast_in_dim.31), calls=%async_computation.1 | async-start | bytes 32768 | tf_op jit(solution)/shard_map/all_to_all | solution.py:36
  236.0 40.0 %all-gather.5.cloned.1.call-start = ((), (), s32[]{:S(2)}) async-start(), calls=%async_computation.7 | async-start | bytes 1114112 | tf_op jit(solution)/shard_map/all_gather | solution.py:149
  246.0 30.0 %all-to-all-start.3 = ((bf16[128,32,16]{0,2,1:T(8,128)(2,1)}), bf16[128,32,16]{0,2,1:T(8,128)(2,1)S(1)}, u32[]{:S(2)}, u32[]{:S(2)}) async-start(bf16[128,32,16]{0,2,1:T(8,128)(2,1)} %bitcast.21), calls=%async_computation.5 | async-start | bytes 262144 | tf_op jit(solution)/shard_map/all_to_all | solution.py:184
Sparse Core Ops, SparseCore 0:
  25.3 46.9 all-gather.2
  244.3 31.6 all-gather.4
Sparse Core Ops, SparseCore 1:
  135.1 14.9 reduce-scatter.2
  203.3 40.1 reduce-scatter.4
where the time goes:
time: 294 us; the launch traced here: 289 us
  waiting for transfers between devices  82.1 us (28%)
  local copies, waits for them, and re-layouts  50 us (17%)
  other arithmetic  41.4 us (14%)
  matrix products  35.2 us (12%)
  blocking collectives  35 us (12%)
  starting transfers between devices  28.5 us (10%)
  between operations  16.3 us (6%)
    all_to_all x1, waiting for transfers between devices, sent_and_summed(): lax.all_to_all(split_up(value, dim, devices), axis, 0, 0, tiled=True)  30.3 us
    another operation x4, other arithmetic  25.5 us
    all_gather x1, blocking collectives, gather_turned(): out = lax.all_gather(both, axis, axis=0, tiled=True)  23.8 us
    all_gather x1, waiting for transfers between devices, on_device(): mix_out = lax.all_gather(own_columns, TP, axis=1, tiled=True)  23.3 us
    all_to_all x1, waiting for transfers between devices, on_device(): lax.all_to_all(outgoing, EP, split_axis=0, concat_axis=0, tiled=True)  20.7 us
    dot_general x1, matrix products, stick_terms(): jnp.einsum('hts,shd->thd', weights, value_rows, preferred_element_type=jn...  18.7 us
    another operation x6, local copies, waits for them, and re-layouts  12.5 us
    all_gather x1, blocking collectives, gathered_by_axis(): out = lax.all_gather(out, axes[number], axis=dim, tiled=True)  11.3 us
  transfers between devices with their start and end apart: 8, of which 5 were waited for; matrix products, arithmetic and copies ran while one was open for 35% of the time, Pallas kernels for 0%

commit v1 on v0

--- a/solution.py
+++ b/solution.py
@@ -146,7 +146,9 @@
         out_gain, lax.axis_index(TP) * column_count, column_count, 0
     ).astype(jnp.float32)
     own_columns = (share.T * factor[:, None] * gain_share[None, :]).astype(jnp.bfloat16)
-    mix_out = lax.all_gather(own_columns, TP, axis=1, tiled=True)
+    mix_out = jnp.concatenate(
+        lax.all_to_all(jnp.stack([own_columns] * lax.axis_size(TP)), TP, 0, 0), axis=1
+    )
     token_count, top_count = routes.shape
     ep_count = lax.axis_size(EP)
     experts = w_gate.shape[0] * ep_count

time: 294 us -> 314 us (1.068)
  the two profiles are of different devices: /device:TPU:1 before, /device:TPU:16 now
where the time goes in v1:
time: 314 us; the launch traced here: 308 us
  waiting for transfers between devices  91.9 us (29%)
  local copies, waits for them, and re-layouts  50 us (16%)
  starting transfers between devices  42.8 us (14%)
  other arithmetic  40.7 us (13%)
  matrix products  35.6 us (11%)
  blocking collectives  31.4 us (10%)
  between operations  16.1 us (5%)
    reduce_scatter x1, waiting for transfers between devices, summed_rows_2(): return lax.psum_scatter(tiles, chips, scatter_dimension=0, tiled=True)[0]  41.2 us
    another operation x4, other arithmetic  25.5 us
    all_to_all x1, waiting for transfers between devices, sent_and_summed(): lax.all_to_all(split_up(value, dim, devices), axis, 0, 0, tiled=True)  24.4 us
    dot_general x1, matrix products, stick_terms(): jnp.einsum('hts,shd->thd', weights, value_rows, preferred_element_type=jn...  19.1 us
    all_gather x1, blocking collectives, gather_turned(): out = lax.all_gather(both, axis, axis=0, tiled=True)  18 us
    all_gather x1, blocking collectives, gathered_by_axis(): out = lax.all_gather(out, axes[number], axis=dim, tiled=True)  13.3 us
    all_gather x1, waiting for transfers between devices, gathered_by_axis(): out = lax.all_gather(out, axes[number], axis=dim, tiled=True)  13.3 us
    another operation x6, local copies, waits for them, and re-layouts  12.4 us
  transfers between devices with their start and end apart: 8, of which 5 were waited for; matrix products, arithmetic and copies ran while one was open for 34% of the time, Pallas kernels for 0%

profile of v1, /device:TPU:16, one launch (start us, length us, event | category | flops | bytes accessed | tf_op | source)
XLA Modules:
  0.0 308.5 jit_solution(14282704694856980478)
XLA Ops:
  8.1 1.6 fusion.13
  10.3 1.8 convolution_convert_fusion.3
  12.1 1.8 convolution_convert_fusion.4
  13.9 13.3 %all_gather.9 = bf16[1024,128]{0,1:T(8,128)(2,1)} all-gather(bf16[256,128]{0,1:T(8,128)(2,1)S(1)} %pad_maximum_fusion), channel_id=1, replica_groups=mesh['ep_0'=8,'ep_1'=4,'tp_0'=8,'tp_1'=2] {'ep_1'}, dimensions={0}, use_global_device_ids=true | all-gather | bytes 327680 | tf_op jit(solution)/shard_map/all_gather | solution.py:18
  30.4 2.9 scatter_custom_fusion
  34.3 18.0 %all_gather.11 = bf16[2048,97]{0,1:T(8,128)(2,1)S(1)} all-gather(bf16[128,97]{0,1:T(8,128)(2,1)S(1)} %pad_maximum_fusion.1), channel_id=1, replica_groups=mesh['ep_0'=8,'ep_1'=4,'tp_0'=8,'tp_1'=2] {'tp_0','tp_1'}, dimensions={0}, use_global_device_ids=true | all-gather | bytes 422144 | tf_op jit(solution)/shard_map/all_gather | solution.py:47
  52.6 2.5 gather_fusion
  55.1 1.5 broadcast_select_fusion
  56.6 11.2 %all-to-all-start.3 = ((bf16[32,16,2048]{2,1,0:T(8,128)(2,1)}), bf16[32,16,2048]{2,1,0:T(8,128)(2,1)S(1)}, u32[]{:S(2)}, u32[]{:S(2)}) async-start(bf16[32,16,2048]{2,1,0:T(8,128)(2,1)} %broadcast_select_fusion), calls=%async_computation.3 | async-start | bytes 4194304 | tf_op jit(solution)/shard_map/all_to_all | solution.py:169
  68.2 13.3 %all-gather.2.cloned.1.call-done = bf16[8192,128]{0,1:T(8,128)(2,1)} async-done(((bf16[1024,128]{0,1:T(8,128)(2,1)}), bf16[8192,128]{0,1:T(8,128)(2,1)}) %all-gather.2.cloned.1.call-update) | async-done | bytes 2097168 | tf_op jit(solution)/shard_map/all_gather | solution.py:18
  81.5 7.1 %fusion = f32[256,8192]{1,0:T(8,128)} fusion(f32[8192]{0:T(1024)S(1)} %bitcast.118, bf16[64,2048]{1,0:T(8,128)(2,1)S(1)} %copy-done.3, bf16[8192,128]{0,1:T(8,128)(2,1)} %all-gather.2.cloned.1.call-done, bf16[256,2048]{1,0:T(8,128)(2,1)} %param.15, f32[2048]{0:T(1024)S(1)} %convert_element_type.101, f32[256]{0:T(256)S(1)} %add_rsqrt_fusion.1), kind=kOutput, calls=%fused_computation.6 | convolution fusion | flops 341852160 | bytes 10789888 | tf_op jit(solution)/shard_map/thd,shd->hts/dot_general | solution.py:90
  88.6 7.4 %fusion.9 = f32[32,8,64,128]{3,1,2,0:T(8,128)S(1)} fusion(f32[256,8192]{1,0:T(8,128)} %fusion, s32[256]{0:T(256)S(1)} %iota_add_fusion), kind=kLoop, calls=%fused_computation.17 | loop fusion | flops 18874368 | bytes 16778240
  96.0 4.8 %copy.112 = f32[32,8,64,128]{3,2,1,0:T(8,128)} copy(f32[32,8,64,128]{3,1,2,0:T(8,128)S(1)} %fusion.9) | data formatting | bytes 16777216
  100.9 9.7 %copy.93 = f32[1,256,64,128]{1,2,3,0:T(8,128)} copy(f32[1,256,64,128]{3,2,1,0:T(8,128)} %bitcast.108) | data formatting | bytes 16777216 | tf_op jit(solution)/shard_map/reshape
  110.6 24.0 %fusion.67 = f32[1,256,64,128]{1,2,3,0:T(8,128)} fusion(f32[1,256,64,128]{1,2,3,0:T(8,128)} %copy.93), kind=kOutput, calls=%fused_computation.110 | output fusion | flops 266338304 | bytes 16777216 | tf_op jit(solution)/shard_map/reduce-window
  134.6 8.9 %copy.94 = f32[1,256,64,128]{3,2,1,0:T(8,128)} copy(f32[1,256,64,128]{1,2,3,0:T(8,128)} %fusion.67) | data formatting | bytes 16777216 | tf_op jit(solution)/shard_map/reduce-window
  145.8 4.7 %fusion.12 = bf16[2048,512]{0,1:T(8,128)(2,1)} fusion(bf16[512,2048]{1,0:T(8,128)(2,1)S(1)} %bitcast.110, bf16[1,128,2048]{2,1,0:T(8,128)(2,1)S(1)} %copy-done, bf16[1,2048,128]{2,1,0:T(8,128)(2,1)} %param.28, f32[512,128]{1,0:T(8,128)S(1)} %convolution_minimum_fusion), kind=kOutput, calls=%fused_computation.20 | convolution fusion | flops 538509312 | bytes 5505024 | tf_op jit(solution)/shard_map/dot_general | solution.py:176
  150.5 3.2 %reshape_reshape.3 = bf16[8,2,128,512]{2,1,0,3:T(2,128)(2,1)S(1)} reshape(bf16[2048,512]{0,1:T(8,128)(2,1)} %fusion.12) | data formatting | bytes 4194304 | tf_op jit(solution)/shard_map/reshape;reshape | solution.py:61
  153.7 4.6 %copy.105 = bf16[8,2,128,512]{3,2,0,1:T(8,128)(2,1)} copy(bf16[8,2,128,512]{2,1,0,3:T(2,128)(2,1)S(1)} %reshape_reshape.3) | data formatting | bytes 4194304 | tf_op jit(solution)/shard_map/reshape;reshape | solution.py:61
  158.3 2.3 broadcast.142
  160.7 19.1 %fusion.23 = bf16[256,64]{0,1:T(8,128)(2,1)S(1)} fusion(f32[32,8,64,128]{3,2,1,0:T(8,128)S(1)} %bitcast.113, f32[32,8,64,128]{3,2,1,0:T(8,128)} %bitcast.112, f32[256,8192]{1,0:T(8,128)} %fusion, s32[256]{0:T(256)S(1)} %iota_add_fusion, bf16[8192,128]{0,1:T(8,128)(2,1)S(1)} %copy-done.1), kind=kOutput, calls=%fused_computation.39 | convolution fusion | flops 314589184 | bytes 26248192 | tf_op jit(solution)/shard_map/hts,shd->thd/dot_general | solution.py:99
  181.5 7.8 %all-to-all-start = ((bf16[16,128,256]{1,2,0:T(8,128)(2,1)}), bf16[16,128,256]{1,2,0:T(8,128)(2,1)S(1)}, u32[]{:S(2)}, u32[]{:S(2)}) async-start(bf16[16,128,256]{1,2,0:T(8,128)(2,1)} %bitcast.105), calls=%async_computation | async-start | bytes 2097152 | tf_op jit(solution)/shard_map/all_to_all | solution.py:30
  189.4 24.4 %all-to-all-done = bf16[16,128,256]{1,2,0:T(8,128)(2,1)S(1)} async-done(((bf16[16,128,256]{1,2,0:T(8,128)(2,1)}), bf16[16,128,256]{1,2,0:T(8,128)(2,1)S(1)}, u32[]{:S(2)}, u32[]{:S(2)}) %all-to-all-start) | async-done | bytes 1048608 | tf_op jit(solution)/shard_map/all_to_all | solution.py:30
  214.6 7.0 %all-to-all-start.1 = ((f32[16,1,256]{2,1,0:T(1,128)}), f32[16,1,256]{2,1,0:T(1,128)S(1)}, u32[]{:S(2)}, u32[]{:S(2)}) async-start(f32[16,1,256]{2,1,0:T(1,128)} %broadcast_in_dim.31), calls=%async_computation.1 | async-start | bytes 32768 | tf_op jit(solution)/shard_map/all_to_all | solution.py:36
  222.5 4.6 %all-to-all-done.1 = f32[16,1,256]{2,1,0:T(1,128)S(1)} async-done(((f32[16,1,256]{2,1,0:T(1,128)}), f32[16,1,256]{2,1,0:T(1,128)S(1)}, u32[]{:S(2)}, u32[]{:S(2)}) %all-to-all-start.1) | async-done | bytes 16416 | tf_op jit(solution)/shard_map/all_to_all | solution.py:36
  228.4 5.8 %all-to-all-start.2 = ((bf16[16,256,128]{2,1,0:T(8,128)(2,1)}), bf16[16,256,128]{2,1,0:T(8,128)(2,1)S(1)}, u32[]{:S(2)}, u32[]{:S(2)}) async-start(bf16[16,256,128]{2,1,0:T(8,128)(2,1)} %stack.2), calls=%async_computation.2 | async-start | bytes 2097152 | tf_op jit(solution)/shard_map/all_to_all | solution.py:150
  234.4 41.2 %reduce-scatter.5.cloned.1.call-done = bf16[1,128,512]{2,1,0:T(8,128)(2,1)} async-done(((bf16[8,128,512]{2,1,0:T(8,128)(2,1)}), bf16[1,128,512]{2,1,0:T(8,128)(2,1)}) %reduce-scatter.5.cloned.1.call-update) | async-done | bytes 131088 | tf_op jit(solution)/shard_map/reduce_scatter | solution.py:63
  275.6 1.7 copy.106
  277.3 10.7 %all-to-all-start.4 = ((bf16[128,32,16]{0,2,1:T(8,128)(2,1)}), bf16[128,32,16]{0,2,1:T(8,128)(2,1)S(1)}, u32[]{:S(2)}, u32[]{:S(2)}) async-start(bf16[128,32,16]{0,2,1:T(8,128)(2,1)} %bitcast.23), calls=%async_computation.6 | async-start | bytes 262144 | tf_op jit(solution)/shard_map/all_to_all | solution.py:186
  288.8 1.4 copy.108
  290.2 8.3 %all-to-all-done.4 = bf16[128,32,16]{0,2,1:T(8,128)(2,1)S(1)} async-done(((bf16[128,32,16]{0,2,1:T(8,128)(2,1)}), bf16[128,32,16]{0,2,1:T(8,128)(2,1)S(1)}, u32[]{:S(2)}, u32[]{:S(2)}) %all-to-all-start.4) | async-done | bytes 131104 | tf_op jit(solution)/shard_map/all_to_all | solution.py:186
  298.5 1.4 gather_fusion.1
  (74 shorter events, 14.4 us)
Async XLA Ops:
  8.0 137.8 %copy-start = (bf16[1,128,2048]{2,1,0:T(8,128)(2,1)S(1)}, bf16[1,128,2048]{2,1,0:T(8,128)(2,1)}, u32[]{:S(2)}) copy-start(bf16[1,128,2048]{2,1,0:T(8,128)(2,1)} %param.29) | copy-start | bytes 1572868
  8.0 73.5 %all-gather.2.cloned.1.call-start = ((), (), s32[]{:S(2)}) async-start(), calls=%async_computation.7 | async-start | bytes 2359296 | tf_op jit(solution)/shard_map/all_gather | solution.py:18
  55.1 26.4 %copy-start.3 = (bf16[64,2048]{1,0:T(8,128)(2,1)S(1)}, bf16[64,2048]{1,0:T(8,128)(2,1)}, u32[]{:S(2)}) copy-start(bf16[64,2048]{1,0:T(8,128)(2,1)} %param.17) | copy-start | bytes 786436
  55.1 26.4 %copy-start.5 = (f32[1,8192]{1,0:T(1,128)S(1)}, f32[1,8192]{1,0:T(1,128)}, u32[]{:S(2)}) copy-start(f32[1,8192]{1,0:T(1,128)} %param.20) | copy-start | bytes 98308
  56.6 88.4 %all-to-all-start.3 = ((bf16[32,16,2048]{2,1,0:T(8,128)(2,1)}), bf16[32,16,2048]{2,1,0:T(8,128)(2,1)S(1)}, u32[]{:S(2)}, u32[]{:S(2)}) async-start(bf16[32,16,2048]{2,1,0:T(8,128)(2,1)} %broadcast_select_fusion), calls=%async_computation.3 | async-start | bytes 4194304 | tf_op jit(solution)/shard_map/all_to_all | solution.py:169
  67.8 159.3 %reduce-scatter.3.cloned.1.call-start = ((), (), s32[]{:S(2)}) async-start(), calls=%async_computation.8 | async-start | bytes 3145728 | tf_op jit(solution)/shard_map/reduce_scatter | solution.py:62
  134.6 10.5 %copy-start.2 = (bf16[1,2048,128]{2,1,0:T(8,128)(2,1)S(1)}, bf16[1,2048,128]{2,1,0:T(8,128)(2,1)}, u32[]{:S(2)}) copy-start(bf16[1,2048,128]{2,1,0:T(8,128)(2,1)} %param.27) | copy-start | bytes 1572868
  158.3 2.4 copy-start.1
  160.7 19.1 %copy-start.4 = (bf16[64,2048]{1,0:T(8,128)(2,1)S(1)}, bf16[64,2048]{1,0:T(8,128)(2,1)}, u32[]{:S(2)}) copy-start(bf16[64,2048]{1,0:T(8,128)(2,1)} %param.21) | copy-start | bytes 786436
  179.8 108.2 %copy-start.6 = (s32[96,4]{0,1:T(4,128)S(1)}, s32[96,4]{0,1:T(4,128)}, u32[]{:S(2)}) copy-start(s32[96,4]{0,1:T(4,128)} %param.25) | copy-start | bytes 4612
  179.8 108.3 %copy-start.7 = (f32[96,4]{0,1:T(4,128)S(1)}, f32[96,4]{0,1:T(4,128)}, u32[]{:S(2)}) copy-start(f32[96,4]{0,1:T(4,128)} %param.26) | copy-start | bytes 4612
  181.5 32.2 %all-to-all-start = ((bf16[16,128,256]{1,2,0:T(8,128)(2,1)}), bf16[16,128,256]{1,2,0:T(8,128)(2,1)S(1)}, u32[]{:S(2)}, u32[]{:S(2)}) async-start(bf16[16,128,256]{1,2,0:T(8,128)(2,1)} %bitcast.105), calls=%async_computation | async-start | bytes 2097152 | tf_op jit(solution)/shard_map/all_to_all | solution.py:30
  214.6 12.4 %all-to-all-start.1 = ((f32[16,1,256]{2,1,0:T(1,128)}), f32[16,1,256]{2,1,0:T(1,128)S(1)}, u32[]{:S(2)}, u32[]{:S(2)}) async-start(f32[16,1,256]{2,1,0:T(1,128)} %broadcast_in_dim.31), calls=%async_computation.1 | async-start | bytes 32768 | tf_op jit(solution)/shard_map/all_to_all | solution.py:36
  221.7 54.0 %reduce-scatter.5.cloned.1.call-start = ((), (), s32[]{:S(2)}) async-start(), calls=%async_computation.9 | async-start | bytes 1179648 | tf_op jit(solution)/shard_map/reduce_scatter | solution.py:63
  228.4 48.9 %all-to-all-start.2 = ((bf16[16,256,128]{2,1,0:T(8,128)(2,1)}), bf16[16,256,128]{2,1,0:T(8,128)(2,1)S(1)}, u32[]{:S(2)}, u32[]{:S(2)}) async-start(bf16[16,256,128]{2,1,0:T(8,128)(2,1)} %stack.2), calls=%async_computation.2 | async-start | bytes 2097152 | tf_op jit(solution)/shard_map/all_to_all | solution.py:150
  277.3 21.2 %all-to-all-start.4 = ((bf16[128,32,16]{0,2,1:T(8,128)(2,1)}), bf16[128,32,16]{0,2,1:T(8,128)(2,1)S(1)}, u32[]{:S(2)}, u32[]{:S(2)}) async-start(bf16[128,32,16]{0,2,1:T(8,128)(2,1)} %bitcast.23), calls=%async_computation.6 | async-start | bytes 262144 | tf_op jit(solution)/shard_map/all_to_all | solution.py:186
Sparse Core Ops, SparseCore 0:
  27.4 54.0 all-gather.1
Sparse Core Ops, SparseCore 1:
  158.4 18.2 reduce-scatter.2
  227.3 48.3 reduce-scatter.4
